TPU v7x, 512 devices: a whole 4x8x8 slice. The times are simulated.
512 devices in a mesh: sp: 64 (over z, y), tp: 8 (over x, core).
Axes of the slice: x: 4, y: 8, z: 8, core: 2. Of those that a mesh axis runs over, the one named last changes fastest.
Arguments:
- tokens: bfloat16 [65536, 2048], P(('sp', 'tp')), may hold values from -6 to 6
- norm_gain: float32 [2048], replicated, may hold values from 0.1 to 1.9
- w_query: bfloat16 [2048, 2048], P('sp', 'tp'), may hold values from -0.125 to 0.125
- w_key: bfloat16 [2048, 2048], P('sp', 'tp'), may hold values from -0.125 to 0.125
- w_value: bfloat16 [2048, 4096], P('sp', 'tp'), may hold values from -0.125 to 0.125
- w_rank_down: bfloat16 [2048, 16], replicated, may hold values from -0.125 to 0.125
- w_rank_up: bfloat16 [16, 2048], P(None, 'tp'), may hold values from -1.5 to 1.5
- gate_bias: float32 [2048], P('tp')
- decay_shift: float32 [65536], P('sp'), may hold values from -1 to 0
- out_gain: float32 [512], replicated, may hold values from 0.1 to 1.9
- w_out: bfloat16 [4096, 2048], P('tp', 'sp'), may hold values from -0.09375 to 0.09375
Outputs:
- mixed: bfloat16 [65536, 2048], P(('sp', 'tp'))
All inputs are finite; a program needn't handle non-finite values.
Results may differ from a plain program's by a relative error of at most 0.015.
Values may be sent and summed in bfloat16 or wider, within the bound.
A program may use at most 128 MiB of HBM per device.

v0:
```python
import jax
import jax.numpy as jnp
from jax import lax
from jax.sharding import Mesh
from jax.sharding import PartitionSpec as P

DK = 256
DV = 512
TAU = 16
BLOCK = 64
SP = ("sp_0", "sp_1")
SP_TP = ("sp_0", "sp_1", "tp")
EPS = 1e-06


def sent_together(arrays, axis, dim, along):
    both = jnp.concatenate(arrays, axis=along)
    out, at, finished = (lax.all_gather(both, axis, axis=dim, tiled=True), 0, [])
    for a in arrays:
        finished.append(lax.slice_in_dim(out, at, at + a.shape[along], axis=along))
        at += a.shape[along]
    return tuple(finished)


def filled_with(value, identity):
    return jax.tree.map(
        lambda a, e: jnp.broadcast_to(jnp.asarray(e, a.dtype), a.shape), value, identity
    )


def entering(value, axes, combine, identity):
    before = start = filled_with(value, identity)
    total = value
    for axis in reversed(axes):
        size, mine = (lax.axis_size(axis), lax.axis_index(axis))
        pieces = jax.tree.map(lambda part: lax.all_gather(part, axis), total)
        inside, total = (start, start)
        for k in range(size):
            passed = k < mine
            total = combine(total, jax.tree.map(lambda part: part[k], pieces))
            inside = jax.tree.map(lambda new, old: jnp.where(passed, new, old), total, inside)
        before = combine(inside, before)
    return before


def cut_along(value, dim, size):
    before, after = (value.shape[:dim], value.shape[dim + 1 :])
    return jnp.moveaxis(value.reshape(*before, size, -1, *after), dim, 0)


def sent_and_summed(value, axis, dim):
    size = lax.axis_size(axis)
    parts = lax.all_to_all(cut_along(value, dim, size), axis, 0, 0, tiled=True)
    return jnp.sum(parts.astype(jnp.float32), axis=0)


def rms_rows(values, gain):
    wide = values.astype(jnp.float32)
    return wide * lax.rsqrt(jnp.mean(wide * wide, axis=-1, keepdims=True) + EPS) * gain


def local_pass(query, key, value, log_decay, state):
    rows, heads, width = query.shape
    blocks = rows // BLOCK

    def split(tensor):
        return tensor.reshape((blocks, BLOCK) + tensor.shape[1:])

    causal = jnp.tril(jnp.ones((BLOCK, BLOCK), dtype=bool))

    def local_step(carry, inputs):
        q_blk, k_blk, v_blk, g_blk = inputs
        cumul = jnp.cumsum(g_blk, axis=0)
        centre = cumul - cumul[BLOCK // 2]
        q_scaled = (q_blk * jnp.exp(centre)).astype(jnp.bfloat16)
        k_scaled = (k_blk * jnp.exp(-centre)).astype(jnp.bfloat16)
        scores = jnp.einsum("ihd,jhd->hij", q_scaled, k_scaled, preferred_element_type=jnp.float32)
        scores = jnp.where(causal[None], scores, 0.0).astype(jnp.bfloat16)
        within = jnp.einsum("hij,jhe->ihe", scores, v_blk, preferred_element_type=jnp.float32)
        final = cumul[-1]
        decayed = (k_blk * jnp.exp(final - cumul)).astype(jnp.bfloat16)
        nxt = jnp.exp(final)[:, :, None] * carry + jnp.einsum(
            "jhd,jhe->hde", decayed, v_blk, preferred_element_type=jnp.float32
        )
        return (nxt, (within, q_blk * jnp.exp(cumul), final, carry))

    carry, (within, reach, finals, starts) = lax.scan(
        local_step, state, (split(query), split(key), split(value), split(log_decay))
    )
    return (within, reach, finals, starts, carry)


def state_only(key, value, log_decay, state):
    rows, heads, width = key.shape
    blocks = rows // BLOCK

    def split(tensor):
        return tensor.reshape((blocks, BLOCK) + tensor.shape[1:])

    def state_step(carry, inputs):
        k_blk, v_blk, g_blk = inputs
        cumul = jnp.cumsum(g_blk, axis=0)
        final = cumul[-1]
        decayed = (k_blk * jnp.exp(final - cumul)).astype(jnp.bfloat16)
        carry = jnp.exp(final)[:, :, None] * carry + jnp.einsum(
            "jhd,jhe->hde", decayed, v_blk, preferred_element_type=jnp.float32
        )
        return (carry, final)

    carry, finals = lax.scan(state_step, state, (split(key), split(value), split(log_decay)))
    return (carry, finals)


def read_out(reach, starts):
    blocks, block, heads, width = reach.shape
    result = jnp.einsum(
        "nihd,nhde->nihe",
        reach.astype(jnp.bfloat16),
        starts.astype(jnp.bfloat16),
        preferred_element_type=jnp.float32,
    )
    return result.reshape(blocks * block, heads, -1)


def combine(earlier, later):
    return (earlier[0] * later[0], later[0][:, :, None] * earlier[1] + later[1])


def on_device(
    tokens,
    norm_gain,
    w_query,
    w_key,
    w_value,
    w_rank_down,
    w_rank_up,
    gate_bias,
    decay_shift,
    out_gain,
    w_out,
):
    normed = rms_rows(tokens, norm_gain).astype(jnp.bfloat16)
    query_w, key_w, value_w = sent_together((w_query, w_key, w_value), SP, 0, 1)
    keys_here = query_w.shape[1]
    vals_here = value_w.shape[1]
    heads_here = keys_here // DK
    w_joined = jnp.concatenate([query_w, key_w, value_w, w_rank_down], axis=1)
    joined = jnp.dot(
        lax.all_gather(normed, "tp", axis=0, tiled=True),
        w_joined,
        preferred_element_type=jnp.float32,
    ).astype(jnp.bfloat16)
    span = joined.shape[0]
    q_heads = joined[:, :keys_here].astype(jnp.float32).reshape(span, heads_here, DK) * DK ** (-0.5)
    k_heads = joined[:, keys_here : 2 * keys_here].astype(jnp.float32).reshape(span, heads_here, DK)
    v_heads = joined[:, 2 * keys_here : 2 * keys_here + vals_here].reshape(span, heads_here, DV)
    rank = joined[:, 2 * keys_here + vals_here :]
    pre = jnp.dot(rank, w_rank_up, preferred_element_type=jnp.float32) + gate_bias
    log_decay = (jax.nn.log_sigmoid(pre) / TAU + decay_shift[:, None]).reshape(span, heads_here, DK)
    empty = jnp.zeros((heads_here, DK, DV), jnp.float32)
    identity = (jnp.ones((heads_here, DK), jnp.float32), empty)
    local_end, finals = state_only(k_heads, v_heads, log_decay, empty)
    carried = entering((jnp.exp(jnp.sum(finals, axis=0)), local_end), SP, combine, identity)[1]
    within, reach, _, starts, _ = local_pass(q_heads, k_heads, v_heads, log_decay, carried)
    attended = within.reshape(span, heads_here, DV) + read_out(reach, starts)
    shaped = rms_rows(attended, out_gain).astype(jnp.bfloat16).reshape(span, heads_here * DV)
    out_whole = lax.all_gather(w_out, SP, axis=1, tiled=True)
    return sent_and_summed(
        jnp.dot(shaped, out_whole, preferred_element_type=jnp.float32).astype(jnp.bfloat16), "tp", 0
    ).astype(jnp.bfloat16)


def solution(mesh):
    finer = Mesh(mesh.devices.reshape(8, 8, mesh.shape["tp"]), ("sp_0", "sp_1", "tp"))
    in_specs = (
        P(SP_TP, None),
        P(),
        P(SP, "tp"),
        P(SP, "tp"),
        P(SP, "tp"),
        P(),
        P(None, "tp"),
        P("tp"),
        P(SP),
        P(),
        P("tp", SP),
    )
    out_specs = P(SP_TP, None)
    return jax.shard_map(
        on_device, mesh=finer, in_specs=in_specs, out_specs=out_specs, check_vma=False
    )
```

profile of v0, /device:TPU:1, one launch (start us, length us, event | category | flops | bytes accessed | tf_op | source)
XLA Modules:
  0.0 498.0 jit_solution(9612616746641343713)
XLA Ops:
  7.8 2.0 fusion.61
  12.5 40.7 %all-gather.9.cloned.1.call-done = bf16[1024,2048]{1,0:T(8,128)(2,1)} async-done(((bf16[128,2048]{1,0:T(8,128)(2,1)}), bf16[1024,2048]{1,0:T(8,128)(2,1)}) %all-gather.9.cloned.1.call-update) | async-done | bytes 4194320 | tf_op jit(solution)/shard_map/all_gather | solution.py:149
  53.2 85.4 %all-gather.11.cloned.1.call-done = bf16[2048,1024]{1,0:T(8,128)(2,1)} async-done(((bf16[32,1024]{1,0:T(8,128)(2,1)}), bf16[2048,1024]{1,0:T(8,128)(2,1)}) %all-gather.11.cloned.1.call-update) | async-done | bytes 4194320 | tf_op jit(solution)/shard_map/all_gather | solution.py:18
  138.6 8.1 %fusion.51 = bf16[1024,1040]{0,1:T(8,128)(2,1)S(1)} fusion(bf16[1024,2048]{1,0:T(8,128)(2,1)} %all-gather.9.cloned.1.call-done, bf16[2048,16]{1,0:T(8,128)(2,1)S(1)} %copy.37, bf16[2048,1024]{1,0:T(8,128)(2,1)} %all-gather.11.cloned.1.call-done), kind=kOutput, calls=%fused_computation.62 | convolution fusion | flops 4371660800 | bytes 10584064 | tf_op jit(solution)/shard_map/dot_general | solution.py:148
  148.0 1.9 fusion.64
  149.8 2.5 copy.39
  152.4 3.4 copy.42
  157.3 2.1 copy.43
  160.7 48.5 %while.31 = (s32[]{:T(128)}, f32[1,256,512]{2,1,0:T(8,128)S(1)}, f32[16,1,256]{2,1,0:T(1,128)S(1)}, f32[16,64,1,256]{3,2,1,0:T(1,128)}, f32[16,64,1,256]{3,2,1,0...) while((s32[]{:T(128)}, f32[1,256,512]{2,1,0:T(8,128)S(1)}, ...), condition=%wide.region_3.4_spmd.clone, body=%wide.region_1.3_spmd.clone.sunk | while | flops 18251780 | bytes 1450087 | solution.py:110
  210.2 11.0 %all-gather.2 = f32[8,1,256]{2,1,0:T(1,128)S(1)} all-gather(f32[1,1,256]{2,1,0:T(1,128)S(1)} %bitcast.299), channel_id=2, replica_groups=mesh['sp_0'=8,'sp_1'=8,'tp'=8] {'sp_1'}, dimensions={0}, use_global_device_ids=true | all-gather | bytes 9216 | tf_op jit(solution)/shard_map/all_gather | solution.py:36
  221.2 46.4 %all-gather.17.cloned.1.call-done = f32[8,256,512]{2,1,0:T(8,128)} async-done(((f32[1,256,512]{2,1,0:T(8,128)}), f32[8,256,512]{2,1,0:T(8,128)}) %all-gather.17.cloned.1.call-update) | async-done | bytes 4194320 | tf_op jit(solution)/shard_map/all_gather | solution.py:36
  267.6 3.3 bitcast_add_fusion.1
  271.7 13.7 %all_gather.30 = f32[8,1,256]{2,1,0:T(1,128)S(1)} all-gather(f32[1,1,256]{2,1,0:T(1,128)S(1)} %get-tuple-element.230), channel_id=1, replica_groups=mesh['sp_0'=8,'sp_1'=8,'tp'=8] {'sp_0'}, dimensions={0}, use_global_device_ids=true | all-gather | bytes 9216 | tf_op jit(solution)/shard_map/all_gather | solution.py:36
  285.7 42.6 %all-gather.13.cloned.1.call-done = f32[8,1,256,512]{3,2,1,0:T(8,128)} async-done(((f32[1,1,256,512]{3,2,1,0:T(8,128)}), f32[8,1,256,512]{3,2,1,0:T(8,128)}) %all-gather.13.cloned.1.call-update) | async-done | bytes 4194320 | tf_op jit(solution)/shard_map/all_gather | solution.py:36
  328.3 4.3 fusion.68
  332.6 93.2 %while.30 = (s32[]{:T(128)}, f32[1,256,512]{2,1,0:T(8,128)S(1)}, f32[16,64,1,512]{3,1,2,0:T(8,128)}, bf16[16,64,1,256]{3,1,0,2:T(8,128)(2,1)S(1)}, bf16[16,1,256...) while((s32[]{:T(128)}, f32[1,256,512]{2,1,0:T(8,128)S(1)}, ...), condition=%wide.region_7.8_spmd.clone, body=%wide.region_5.7_spmd.clone.sunk | while | flops 24555520 | bytes 3223153 | solution.py:87
  334.8 1.8 fusion.117
  340.6 1.8 fusion.117
  346.4 1.8 fusion.117
  358.0 1.8 fusion.117
  363.9 1.8 fusion.117
  369.7 1.8 fusion.117
  375.5 1.8 fusion.117
  381.4 1.8 fusion.117
  393.0 1.8 fusion.117
  404.7 1.8 fusion.117
  410.5 1.8 fusion.117
  416.3 1.8 fusion.117
  425.8 3.8 multiply_reduce_fusion
  430.0 4.0 convolution_convert_fusion
  434.0 53.6 %all_to_all.5 = bf16[8,128,2048]{2,1,0:T(8,128)(2,1)} all-to-all(bf16[8,128,2048]{2,1,0:T(8,128)(2,1)S(1)} %bitcast.263), channel_id=1, replica_groups=mesh['sp_0'=8,'sp_1'=8,'tp'=8] {'tp'}, dimensions={0} | all-to-all | bytes 8388608 | tf_op jit(solution)/shard_map/all_to_all | solution.py:53
  487.7 3.8 reduce_sum.42
  (265 shorter events, 129.1 us)
Async XLA Ops:
  6.5 141.4 %copy-start = (bf16[16,256]{1,0:T(8,128)(2,1)S(1)}, bf16[16,256]{1,0:T(8,128)(2,1)}, u32[]{:S(2)}) copy-start(bf16[16,256]{1,0:T(8,128)(2,1)} %param.21) | copy-start | bytes 24580
  6.5 46.7 %all-gather.9.cloned.1.call-start = ((), (), s32[]{:S(2)}) async-start(), calls=%async_computation.1 | async-start | bytes 4718592 | tf_op jit(solution)/shard_map/all_gather | solution.py:149
  9.8 128.8 %all-gather.11.cloned.1.call-start = ((), (), s32[]{:S(2)}) async-start(), calls=%async_computation.2 | async-start | bytes 4259840 | tf_op jit(solution)/shard_map/all_gather | solution.py:18
  11.3 256.3 %all-gather.17.cloned.1.call-start = ((), (), s32[]{:S(2)}) async-start(), calls=%async_computation.5 | async-start | bytes 4718592 | tf_op jit(solution)/shard_map/all_gather | solution.py:36
  12.5 135.5 %copy-start.6 = (f32[1024]{0:T(1024)S(1)}, f32[1024]{0:T(1024)}, u32[]{:S(2)}) copy-start(f32[1024]{0:T(1024)} %param.23) | copy-start | bytes 12292
  12.5 135.4 %copy-start.7 = (f32[256]{0:T(256)S(1)}, f32[256]{0:T(256)}, u32[]{:S(2)}) copy-start(f32[256]{0:T(256)} %param.22) | copy-start | bytes 3076
  146.7 5.6 %copy-start.2 = (bf16[1024,1040]{0,1:T(8,128)(2,1)}, bf16[1024,1040]{0,1:T(8,128)(2,1)S(1)}, u32[]{:S(2)}) copy-start(bf16[1024,1040]{0,1:T(8,128)(2,1)S(1)} %fusion.51) | copy-start | bytes 6389764
  152.4 7.1 %slice-start = ((bf16[1024,1040]{0,1:T(8,128)(2,1)}), bf16[1024,512]{0,1:T(8,128)(2,1)S(1)}, s32[]{:S(2)}) async-start(bf16[1024,1040]{0,1:T(8,128)(2,1)} %copy-done.2), calls=%async_computation.6 | async-start | bytes 2097152 | tf_op jit(solution)/shard_map/slice | solution.py:156
  209.2 0.8 copy-start.1
  209.2 62.3 %copy-start.3 = (bf16[1024,1040]{0,1:T(8,128)(2,1)S(1)}, bf16[1024,1040]{0,1:T(8,128)(2,1)}, u32[]{:S(2)}) copy-start(bf16[1024,1040]{0,1:T(8,128)(2,1)} %copy-done.2) | copy-start | bytes 6389764
  210.0 118.2 %all-gather.13.cloned.1.call-start = ((), (), s32[]{:S(2)}) async-start(), calls=%async_computation.3 | async-start | bytes 4718592 | tf_op jit(solution)/shard_map/all_gather | solution.py:36
  270.9 159.1 %all-gather.15.cloned.1.call-start = ((), (), s32[]{:S(2)}) async-start(), calls=%async_computation.4 | async-start | bytes 2129920 | tf_op jit(solution)/shard_map/all_gather | solution.py:167
  328.3 4.3 copy-start.4
  425.8 3.9 copy-start.5
Sparse Core Ops, SparseCore 0:
  10.0 43.2 all-gather.8
  56.3 82.2 all-gather.10
  210.2 57.3 all-gather.16
  271.0 57.2 all-gather.12
  331.2 77.5 all-gather.14
where the time goes:
time: 504 us; the launch traced here: 498 us
  waiting for transfers between devices  216 us (43%)
  matrix products  82.2 us (16%)
  other arithmetic  81 us (16%)
  blocking collectives  78.3 us (16%)
  local copies, waits for them, and re-layouts  25.8 us (5%)
  between operations  13.4 us (3%)
    all_gather x2, waiting for transfers between devices, entering(): pieces = jax.tree.map(lambda part: lax.all_gather(part, axis), total)  89 us
    all_gather x1, waiting for transfers between devices, sent_together(): lax.all_gather(both, axis, axis=dim, tiled=True)  85.4 us
    all_to_all x1, blocking collectives, sent_and_summed(): parts = lax.all_to_all(cut_along(value, dim, size), axis, 0, 0, tiled=True)  53.6 us
    all_gather x1, waiting for transfers between devices, on_device(): lax.all_gather(normed, 'tp', axis=0, tiled=True)  40.7 us
    dot_general x16, matrix products, local_step(): jnp.einsum('hij,jhe->ihe', scores, v_blk, preferred_element_type=jnp.floa...  28.5 us
    all_gather x2, blocking collectives, entering(): pieces = jax.tree.map(lambda part: lax.all_gather(part, axis), total)  24.7 us
    dot_general x16, matrix products, local_step(): jnp.einsum('jhd,jhe->hde', decayed, v_blk, preferred_element_type=jnp.flo...  18.3 us
    dot_general x16, matrix products, state_step(): jnp.einsum('jhd,jhe->hde', decayed, v_blk, preferred_element_type=jnp.flo...  17.7 us
  transfers between devices with their start and end apart: 5, of which 4 were waited for; matrix products, arithmetic and copies ran while one was open for 21% of the time, Pallas kernels for 0%

commit v1 on v0

--- a/solution.py
+++ b/solution.py
@@ -11,6 +11,14 @@
 SP = ("sp_0", "sp_1")
 SP_TP = ("sp_0", "sp_1", "tp")
 EPS = 1e-06
+
+
+def gather_by_exchange(shard, axis, dim):
+    size = lax.axis_size(axis)
+    repeats = [size if d == dim else 1 for d in range(shard.ndim)]
+    return lax.all_to_all(
+        jnp.tile(shard, repeats), axis, split_axis=dim, concat_axis=dim, tiled=True
+    )
 
 
 def sent_together(arrays, axis, dim, along):
@@ -146,9 +154,7 @@
     heads_here = keys_here // DK
     w_joined = jnp.concatenate([query_w, key_w, value_w, w_rank_down], axis=1)
     joined = jnp.dot(
-        lax.all_gather(normed, "tp", axis=0, tiled=True),
-        w_joined,
-        preferred_element_type=jnp.float32,
+        gather_by_exchange(normed, "tp", 0), w_joined, preferred_element_type=jnp.float32
     ).astype(jnp.bfloat16)
     span = joined.shape[0]
     q_heads = joined[:, :keys_here].astype(jnp.float32).reshape(span, heads_here, DK) * DK ** (-0.5)

time: 504 us -> 464 us (0.921)
  waiting for transfers between devices: 216 us -> 164 us
  starting transfers between devices: 0.17 us -> 11.5 us
    all_gather x1, waiting for transfers between devices: 85.4 us -> 25.4 us  [sent_together(): lax.all_gather(both, axis, axis=dim, tiled=True)]
    all_to_all x0 -> x1, waiting for transfers between devices: none -> 48.5 us  [gather_by_exchange(): lax.all_to_all(jnp.tile(shard, repeats), axis, split_axis=dim, concat_axi...]
    all_gather x1 -> x0, waiting for transfers between devices: 40.7 us -> none  [on_device(): lax.all_gather(normed, 'tp', axis=0, tiled=True)]
    all_to_all x0 -> x1, starting transfers between devices: none -> 11.4 us  [gather_by_exchange(): lax.all_to_all(jnp.tile(shard, repeats), axis, split_axis=dim, concat_axi...]
  transfers between devices with their start and end apart: 5 -> 5, of which waited for: 4 -> 4; matrix products, arithmetic and copies ran while one was open for 21% -> 23% of each run, Pallas kernels for 0% -> 0%
where the time goes in v1:
time: 464 us; the launch traced here: 458 us
  waiting for transfers between devices  164 us (35%)
  matrix products  82.2 us (18%)
  other arithmetic  80.2 us (17%)
  blocking collectives  78.3 us (17%)
  local copies, waits for them, and re-layouts  27.5 us (6%)
  between operations  13.4 us (3%)
  starting transfers between devices  11.5 us (2%)
    all_gather x2, waiting for transfers between devices, entering(): pieces = jax.tree.map(lambda part: lax.all_gather(part, axis), total)  89 us
    all_to_all x1, blocking collectives, sent_and_summed(): parts = lax.all_to_all(cut_along(value, dim, size), axis, 0, 0, tiled=True)  53.6 us
    all_to_all x1, waiting for transfers between devices, gather_by_exchange(): lax.all_to_all(jnp.tile(shard, repeats), axis, split_axis=dim, concat_axi...  48.5 us
    dot_general x16, matrix products, local_step(): jnp.einsum('hij,jhe->ihe', scores, v_blk, preferred_element_type=jnp.floa...  28.5 us
    all_gather x1, waiting for transfers between devices, sent_together(): lax.all_gather(both, axis, axis=dim, tiled=True)  25.4 us
    all_gather x2, blocking collectives, entering(): pieces = jax.tree.map(lambda part: lax.all_gather(part, axis), total)  24.7 us
    dot_general x16, matrix products, local_step(): jnp.einsum('jhd,jhe->hde', decayed, v_blk, preferred_element_type=jnp.flo...  18.3 us
    dot_general x16, matrix products, state_step(): jnp.einsum('jhd,jhe->hde', decayed, v_blk, preferred_element_type=jnp.flo...  17.7 us
  transfers between devices with their start and end apart: 5, of which 4 were waited for; matrix products, arithmetic and copies ran while one was open for 23% of the time, Pallas kernels for 0%

profile of v1, /device:TPU:1, one launch (start us, length us, event | category | flops | bytes accessed | tf_op | source)
XLA Modules:
  0.0 458.0 jit_solution(4430962109284820241)
XLA Ops:
  10.4 2.5 tile.2
  12.9 11.4 %all-to-all-start = ((bf16[8,128,2048]{2,1,0:T(8,128)(2,1)}), bf16[8,128,2048]{2,1,0:T(8,128)(2,1)}, u32[]{:S(2)}, u32[]{:S(2)}) async-start(bf16[8,128,2048]{2,1,0:T(8,128)(2,1)} %tile.2), calls=%async_computation | async-start | bytes 8388608 | tf_op jit(solution)/shard_map/all_to_all | solution.py:19
  24.6 48.5 %all-to-all-done = bf16[8,128,2048]{2,1,0:T(8,128)(2,1)} async-done(((bf16[8,128,2048]{2,1,0:T(8,128)(2,1)}), bf16[8,128,2048]{2,1,0:T(8,128)(2,1)}, u32[]{:S(2)}, u32[]{:S(2)}) %all-to-all-start) | async-done | bytes 4194336 | tf_op jit(solution)/shard_map/all_to_all | solution.py:19
  73.2 25.4 %all-gather.8.cloned.1.call-done = bf16[2048,1024]{1,0:T(8,128)(2,1)} async-done(((bf16[32,1024]{1,0:T(8,128)(2,1)}), bf16[2048,1024]{1,0:T(8,128)(2,1)}) %all-gather.8.cloned.1.call-update) | async-done | bytes 4194320 | tf_op jit(solution)/shard_map/all_gather | solution.py:26
  98.6 8.1 %fusion.51 = bf16[1024,1040]{0,1:T(8,128)(2,1)S(1)} fusion(bf16[1024,2048]{1,0:T(8,128)(2,1)} %bitcast, bf16[2048,16]{1,0:T(8,128)(2,1)S(1)} %copy.37, bf16[2048,1024]{1,0:T(8,128)(2,1)} %all-gather.8.cloned.1.call-done), kind=kOutput, calls=%fused_computation.62 | convolution fusion | flops 4371660800 | bytes 10584064 | tf_op jit(solution)/shard_map/dot_general | solution.py:156
  107.9 1.9 fusion.64
  109.8 2.5 copy.39
  112.3 3.4 copy.42
  117.3 2.1 copy.43
  120.7 48.5 %while.31 = (s32[]{:T(128)}, f32[1,256,512]{2,1,0:T(8,128)S(1)}, f32[16,1,256]{2,1,0:T(1,128)S(1)}, f32[16,64,1,256]{3,2,1,0:T(1,128)}, f32[16,64,1,256]{3,2,1,0...) while((s32[]{:T(128)}, f32[1,256,512]{2,1,0:T(8,128)S(1)}, ...), condition=%wide.region_3.4_spmd.clone, body=%wide.region_1.3_spmd.clone.sunk | while | flops 18251780 | bytes 1450087 | solution.py:118
  170.1 11.0 %all-gather.2 = f32[8,1,256]{2,1,0:T(1,128)S(1)} all-gather(f32[1,1,256]{2,1,0:T(1,128)S(1)} %bitcast.300), channel_id=2, replica_groups=mesh['sp_0'=8,'sp_1'=8,'tp'=8] {'sp_1'}, dimensions={0}, use_global_device_ids=true | all-gather | bytes 9216 | tf_op jit(solution)/shard_map/all_gather | solution.py:44
  181.2 46.4 %all-gather.14.cloned.1.call-done = f32[8,256,512]{2,1,0:T(8,128)} async-done(((f32[1,256,512]{2,1,0:T(8,128)}), f32[8,256,512]{2,1,0:T(8,128)}) %all-gather.14.cloned.1.call-update) | async-done | bytes 4194320 | tf_op jit(solution)/shard_map/all_gather | solution.py:44
  227.6 3.3 bitcast_add_fusion.1
  231.6 13.7 %all_gather.26 = f32[8,1,256]{2,1,0:T(1,128)S(1)} all-gather(f32[1,1,256]{2,1,0:T(1,128)S(1)} %get-tuple-element.230), channel_id=1, replica_groups=mesh['sp_0'=8,'sp_1'=8,'tp'=8] {'sp_0'}, dimensions={0}, use_global_device_ids=true | all-gather | bytes 9216 | tf_op jit(solution)/shard_map/all_gather | solution.py:44
  245.7 42.6 %all-gather.10.cloned.1.call-done = f32[8,1,256,512]{3,2,1,0:T(8,128)} async-done(((f32[1,1,256,512]{3,2,1,0:T(8,128)}), f32[8,1,256,512]{3,2,1,0:T(8,128)}) %all-gather.10.cloned.1.call-update) | async-done | bytes 4194320 | tf_op jit(solution)/shard_map/all_gather | solution.py:44
  288.3 4.3 fusion.68
  292.6 93.2 %while.30 = (s32[]{:T(128)}, f32[1,256,512]{2,1,0:T(8,128)S(1)}, f32[16,64,1,512]{3,1,2,0:T(8,128)}, bf16[16,64,1,256]{3,1,0,2:T(8,128)(2,1)S(1)}, bf16[16,1,256...) while((s32[]{:T(128)}, f32[1,256,512]{2,1,0:T(8,128)S(1)}, ...), condition=%wide.region_7.8_spmd.clone, body=%wide.region_5.7_spmd.clone.sunk | while | flops 24555520 | bytes 3223153 | solution.py:95
  294.7 1.8 fusion.117
  300.6 1.8 fusion.117
  306.4 1.8 fusion.117
  318.0 1.8 fusion.117
  323.9 1.8 fusion.117
  329.7 1.8 fusion.117
  335.5 1.8 fusion.117
  341.3 1.8 fusion.117
  353.0 1.8 fusion.117
  364.6 1.8 fusion.117
  376.3 1.8 fusion.117
  385.8 3.8 multiply_reduce_fusion
  390.0 4.0 convolution_convert_fusion
  394.0 53.6 %all_to_all.14 = bf16[8,128,2048]{2,1,0:T(8,128)(2,1)} all-to-all(bf16[8,128,2048]{2,1,0:T(8,128)(2,1)S(1)} %bitcast.264), channel_id=1, replica_groups=mesh['sp_0'=8,'sp_1'=8,'tp'=8] {'tp'}, dimensions={0} | all-to-all | bytes 8388608 | tf_op jit(solution)/shard_map/all_to_all | solution.py:61
  447.6 3.8 reduce_sum.42
  (267 shorter events, 131.2 us)
Async XLA Ops:
  6.5 101.4 %copy-start = (bf16[16,256]{1,0:T(8,128)(2,1)S(1)}, bf16[16,256]{1,0:T(8,128)(2,1)}, u32[]{:S(2)}) copy-start(bf16[16,256]{1,0:T(8,128)(2,1)} %param.21) | copy-start | bytes 24580
  6.5 92.0 %all-gather.8.cloned.1.call-start = ((), (), s32[]{:S(2)}) async-start(), calls=%async_computation.2 | async-start | bytes 4259840 | tf_op jit(solution)/shard_map/all_gather | solution.py:26
  12.9 11.4 %copy-start.5 = (bf16[2048,16]{0,1:T(8,128)(2,1)S(1)}, bf16[2048,16]{0,1:T(8,128)(2,1)}, u32[]{:S(2)}) copy-start(bf16[2048,16]{0,1:T(8,128)(2,1)} %param.20) | copy-start | bytes 196612
  12.9 60.2 %all-to-all-start = ((bf16[8,128,2048]{2,1,0:T(8,128)(2,1)}), bf16[8,128,2048]{2,1,0:T(8,128)(2,1)}, u32[]{:S(2)}, u32[]{:S(2)}) async-start(bf16[8,128,2048]{2,1,0:T(8,128)(2,1)} %tile.2), calls=%async_computation | async-start | bytes 8388608 | tf_op jit(solution)/shard_map/all_to_all | solution.py:19
  24.3 203.2 %all-gather.14.cloned.1.call-start = ((), (), s32[]{:S(2)}) async-start(), calls=%async_computation.5 | async-start | bytes 4718592 | tf_op jit(solution)/shard_map/all_gather | solution.py:44
  98.6 9.4 %copy-start.7 = (f32[1024]{0:T(1024)S(1)}, f32[1024]{0:T(1024)}, u32[]{:S(2)}) copy-start(f32[1024]{0:T(1024)} %param.23) | copy-start | bytes 12292
  98.6 9.4 %copy-start.8 = (f32[256]{0:T(256)S(1)}, f32[256]{0:T(256)}, u32[]{:S(2)}) copy-start(f32[256]{0:T(256)} %param.22) | copy-start | bytes 3076
  106.7 5.6 %copy-start.2 = (bf16[1024,1040]{0,1:T(8,128)(2,1)}, bf16[1024,1040]{0,1:T(8,128)(2,1)S(1)}, u32[]{:S(2)}) copy-start(bf16[1024,1040]{0,1:T(8,128)(2,1)S(1)} %fusion.51) | copy-start | bytes 6389764
  112.3 7.1 %slice-start = ((bf16[1024,1040]{0,1:T(8,128)(2,1)}), bf16[1024,512]{0,1:T(8,128)(2,1)S(1)}, s32[]{:S(2)}) async-start(bf16[1024,1040]{0,1:T(8,128)(2,1)} %copy-done.2), calls=%async_computation.6 | async-start | bytes 2097152 | tf_op jit(solution)/shard_map/slice | solution.py:162
  169.2 0.8 copy-start.1
  169.2 62.3 %copy-start.3 = (bf16[1024,1040]{0,1:T(8,128)(2,1)S(1)}, bf16[1024,1040]{0,1:T(8,128)(2,1)}, u32[]{:S(2)}) copy-start(bf16[1024,1040]{0,1:T(8,128)(2,1)} %copy-done.2) | copy-start | bytes 6389764
  170.0 118.2 %all-gather.10.cloned.1.call-start = ((), (), s32[]{:S(2)}) async-start(), calls=%async_computation.3 | async-start | bytes 4718592 | tf_op jit(solution)/shard_map/all_gather | solution.py:44
  230.9 159.1 %all-gather.12.cloned.1.call-start = ((), (), s32[]{:S(2)}) async-start(), calls=%async_computation.4 | async-start | bytes 2129920 | tf_op jit(solution)/shard_map/all_gather | solution.py:173
  288.3 4.3 copy-start.4
  385.8 3.9 copy-start.6
Sparse Core Ops, SparseCore 0:
  10.4 88.1 all-gather.7
  170.1 57.3 all-gather.13
  231.0 57.2 all-gather.9
  291.2 77.5 all-gather.11
